TPU v7x, 32 devices: a whole 2x2x4 slice. The times are simulated.
32 devices in a mesh: rep: 2 (over x), fs: 8 (over z, y), tp: 2 (over core).
Axes of the slice: x: 2, y: 2, z: 4, core: 2. Of those that a mesh axis runs over, the one named last changes fastest.
Arguments:
- inputs: bfloat16 [8192, 2048], P(('rep', 'fs')), may hold values from -6 to 6
- gain: float32 [2048], replicated, may hold values from 0.1 to 1.9
- gate_weight: bfloat16 [2048, 3072], P('fs', 'tp'), may hold values from -0.125 to 0.125
- up_weight: bfloat16 [2048, 3072], P('fs', 'tp'), may hold values from -0.125 to 0.125
- down_weight: bfloat16 [2048, 3072], P('fs', 'tp'), may hold values from -0.109375 to 0.109375
- cotangent: bfloat16 [8192, 2048], P(('rep', 'fs')), may hold values from -6 to 6
Outputs:
- input_gradient: bfloat16 [8192, 2048], P(('rep', 'fs'))
- gain_gradient: float32 [2048], replicated
- d_down: float32 [2048, 3072], P('fs', 'tp')
All inputs are finite; a program needn't handle non-finite values.
Results may differ from a plain program's by a relative error of at most 0.014.
Values may be sent and summed in bfloat16 or wider, within the bound.
A program may use at most 128 MiB of HBM per device.

v0:
```python
import jax
import jax.numpy as jnp
from jax import lax
from jax.sharding import PartitionSpec as P

EPS = 1e-06


def local(inputs, gain, gate_weight, up_weight, down_weight, cotangent):
    single_precision = inputs.astype(jnp.float32)
    reciprocal_root_mean = lax.rsqrt(
        jnp.mean(single_precision * single_precision, axis=-1, keepdims=True) + EPS
    )
    unit_input = single_precision * reciprocal_root_mean
    normalized_input = (unit_input * gain).astype(jnp.bfloat16)
    row_count = inputs.shape[0]
    contract_cols = (((1,), (1,)), ((), ()))
    gate_full, up_full, down_full = (
        lax.all_gather(gate_weight, "fs", axis=0, tiled=True),
        lax.all_gather(up_weight, "fs", axis=0, tiled=True),
        lax.all_gather(down_weight, "fs", axis=0, tiled=True),
    )
    gate = jnp.dot(normalized_input, gate_full, preferred_element_type=jnp.float32)
    up_proj = jnp.dot(normalized_input, up_full, preferred_element_type=jnp.float32)
    down_sum = jnp.dot(cotangent, down_full, preferred_element_type=jnp.float32)
    gate_sig = jax.nn.sigmoid(gate)
    active = gate * gate_sig
    hidden = (active * up_proj).astype(jnp.bfloat16)
    d_hidden = 0.5 * down_sum
    d_gate = (d_hidden * up_proj * gate_sig * (1.0 + gate * (1.0 - gate_sig))).astype(jnp.bfloat16)
    d_up = (d_hidden * active).astype(jnp.bfloat16)
    partial_value = lax.dot_general(
        d_gate, gate_full, contract_cols, preferred_element_type=jnp.float32
    ) + lax.dot_general(d_up, up_full, contract_cols, preferred_element_type=jnp.float32)
    summed_units = lax.psum(partial_value.astype(jnp.bfloat16), "tp")
    normalized_gradient = summed_units.astype(jnp.float32)
    gain_gradient = lax.psum(jnp.sum(normalized_gradient * unit_input, axis=0), ("rep", "fs"))
    gain_scaled = gain * normalized_gradient
    mean_correction = jnp.mean(gain_scaled * unit_input, axis=-1, keepdims=True)
    input_gradient = (
        cotangent.astype(jnp.float32)
        + reciprocal_root_mean * (gain_scaled - unit_input * mean_correction)
    ).astype(jnp.bfloat16)
    contract_rows = (((0,), (0,)), ((), ()))
    width = cotangent.shape[1]
    groups_fs = lax.axis_size("fs")
    groups_rep = lax.axis_size("rep")
    sub_rows = width // (groups_fs * groups_rep)
    reordered = (
        cotangent.reshape(row_count, groups_fs, groups_rep, sub_rows)
        .transpose(0, 2, 1, 3)
        .reshape(row_count, width)
    )
    summed = lax.psum_scatter(
        0.5 * lax.dot_general(reordered, hidden, contract_rows, preferred_element_type=jnp.float32),
        ("rep", "fs"),
        scatter_dimension=0,
        tiled=True,
    )
    d_down = lax.all_gather(summed, "rep", axis=0, tiled=True)
    return (input_gradient, gain_gradient, d_down)


def solution(mesh):
    placed = (
        P(("rep", "fs"), None),
        P(),
        P("fs", "tp"),
        P("fs", "tp"),
        P("fs", "tp"),
        P(("rep", "fs"), None),
    )
    return jax.shard_map(
        local,
        mesh=mesh,
        in_specs=placed,
        out_specs=(P(("rep", "fs"), None), P(), P("fs", "tp")),
        check_vma=False,
    )
```

profile of v0, /device:TPU:0, one launch (start us, length us, event | category | flops | bytes accessed | tf_op | source)
XLA Modules:
  0.0 600.7 jit_solution(4841965839708579481)
XLA Ops:
  7.2 0.0 copy-start.1
  7.2 0.0 all-gather.9.cloned.1.call-start
  7.2 0.7 all-gather.9.cloned.1.call-update
  7.9 0.0 all-gather.7.cloned.1.call-start
  8.0 0.7 all-gather.7.cloned.1.call-update
  8.7 0.0 all-gather.5.cloned.1.call-start
  8.7 0.7 all-gather.5.cloned.1.call-update
  9.4 0.0 reduce-scatter.2.cloned.1.call-start
  9.5 2.5 copy.11
  12.0 3.3 copy.12
  15.2 0.5 fusion.9
  15.7 95.9 %all-gather.9.cloned.1.call-done = bf16[2048,1536]{1,0:T(8,128)(2,1)} async-done(((bf16[256,1536]{1,0:T(8,128)(2,1)}), bf16[2048,1536]{1,0:T(8,128)(2,1)}) %all-gather.9.cloned.1.call-update) | async-done | bytes 6291472 | tf_op jit(solution)/shard_map/all_gather | solution.py:19
  111.6 7.9 %fusion.14 = f32[512,1536]{1,0:T(8,128)} fusion(bf16[2048,1536]{1,0:T(8,128)(2,1)} %all-gather.9.cloned.1.call-done, bf16[512,2048]{1,0:T(8,128)(2,1)S(1)} %copy-done, f32[2048]{0:T(1024)S(1)} %copy-done.3, f32[512]{0:T(512)S(1)} %add_rsqrt_fusion), kind=kOutput, calls=%fused_computation.25 | convolution fusion | flops 3225419776 | bytes 11544576 | tf_op jit(solution)/shard_map/dot_general | solution.py:23
  119.5 91.2 %all-gather.7.cloned.1.call-done = bf16[2048,1536]{1,0:T(8,128)(2,1)} async-done(((bf16[256,1536]{1,0:T(8,128)(2,1)}), bf16[2048,1536]{1,0:T(8,128)(2,1)}) %all-gather.7.cloned.1.call-update) | async-done | bytes 6291472 | tf_op jit(solution)/shard_map/all_gather | solution.py:20
  210.7 5.8 fusion.16
  216.5 1.7 copy-done.6
  218.2 6.8 %multiply_bitcast_fusion = f32[2048,1536]{0,1:T(8,128)} fusion(bf16[512,2048]{0,1:T(8,128)(2,1)S(1)} %bitcast.14, f32[512,1536]{1,0:T(8,128)S(1)} %fusion.16, f32[512,1536]{1,0:T(8,128)S(1)} %copy-done.4), kind=kOutput, calls=%fused_computation | convolution fusion | flops 3229089792 | bytes 20971520 | tf_op jit(solution)/shard_map/dot_general | solution.py:55
  225.1 0.0 reduce-scatter.2.cloned.1.call-update
  225.1 0.2 all-reduce.2.cloned.1.call-start
  225.3 84.5 %all-gather.5.cloned.1.call-done = bf16[2048,1536]{1,0:T(8,128)(2,1)} async-done(((bf16[256,1536]{1,0:T(8,128)(2,1)}), bf16[2048,1536]{1,0:T(8,128)(2,1)}) %all-gather.5.cloned.1.call-update) | async-done | bytes 6291472 | tf_op jit(solution)/shard_map/all_gather | solution.py:21
  309.8 8.6 %convolution_multiply_fusion = f32[512,1536]{1,0:T(8,128)} fusion(bf16[512,2048]{1,0:T(8,128)(2,1)} %param.11, bf16[2048,1536]{1,0:T(8,128)(2,1)} %all-gather.5.cloned.1.call-done), kind=kOutput, calls=%fused_computation.17 | convolution fusion | flops 3222011904 | bytes 11534336 | tf_op jit(solution)/shard_map/dot_general | solution.py:25
  318.4 8.6 %fusion.12 = f32[512,2048]{1,0:T(8,128)S(1)} fusion(bf16[2048,1536]{1,0:T(8,128)(2,1)} %all-gather.9.cloned.1.call-done, f32[512,1536]{1,0:T(8,128)S(1)} %copy-done.5, f32[512,1536]{1,0:T(8,128)} %convolution_multiply_fusion, f32[512,1536]{1,0:T(8,128)S(1)} %copy-done.7), kind=kOutput, calls=%fused_computation.23 | convolution fusion | flops 3229089792 | bytes 19922944 | tf_op jit(solution)/shard_map/dot_general | solution.py:32
  327.1 6.6 %add_convert_fusion = bf16[512,2048]{1,0:T(8,128)(2,1)} fusion(f32[512,2048]{1,0:T(8,128)S(1)} %fusion.12, bf16[2048,1536]{1,0:T(8,128)(2,1)S(1)} %bitcast.16, f32[512,1536]{1,0:T(8,128)} %convolution_multiply_fusion, f32[512,1536]{1,0:T(8,128)S(1)} %copy-done.5), kind=kOutput, calls=%fused_computation.16 | convolution fusion | flops 3228041216 | bytes 18874368 | tf_op jit(solution)/shard_map/dot_general | solution.py:34
  333.7 0.0 all-reduce.2.cloned.1.call-update
  333.7 0.0 all-gather.11.cloned.1.call-start
  333.7 182.3 %reduce-scatter.2.cloned.1.call-done = f32[128,1536]{0,1:T(8,128)} async-done(((f32[2048,1536]{0,1:T(8,128)}), f32[128,1536]{0,1:T(8,128)}) %reduce-scatter.2.cloned.1.call-update) | async-done | bytes 786448 | tf_op jit(solution)/shard_map/reduce_scatter | solution.py:54
  516.0 0.0 all-gather.11.cloned.1.call-update
  516.1 23.6 %all-reduce.2.cloned.1.call-done = bf16[512,2048]{1,0:T(8,128)(2,1)} async-done(((bf16[512,2048]{1,0:T(8,128)(2,1)}), bf16[512,2048]{1,0:T(8,128)(2,1)}) %all-reduce.2.cloned.1.call-update) | async-done | bytes 2097168 | tf_op jit(solution)/shard_map/psum | solution.py:35
  539.6 2.9 fusion.10
  542.5 43.3 %psum.15 = f32[2048]{0:T(1024)} all-reduce(f32[2048]{0:T(1024)S(1)} %get-tuple-element.12), channel_id=1, replica_groups=mesh['rep'=2,'fs'=8,'tp'=2] {'rep','fs'}, use_global_device_ids=true, to_apply=%region_4.0 | all-reduce | flops 2048 | bytes 16384 | tf_op jit(solution)/shard_map/psum | solution.py:37
  585.8 5.0 fusion.6
  590.8 3.0 copy.13
  (22 shorter events, 0.0 us)
Async XLA Ops:
  7.2 2.3 copy-start.1
  7.2 104.4 %all-gather.9.cloned.1.call-start = ((), (), s32[]{:S(2)}) async-start(), calls=%async_computation.3 | async-start | bytes 7077888 | tf_op jit(solution)/shard_map/all_gather | solution.py:19
  7.9 202.8 %all-gather.7.cloned.1.call-start = ((), (), s32[]{:S(2)}) async-start(), calls=%async_computation.2 | async-start | bytes 7077888 | tf_op jit(solution)/shard_map/all_gather | solution.py:20
  8.7 301.1 %all-gather.5.cloned.1.call-start = ((), (), s32[]{:S(2)}) async-start(), calls=%async_computation.1 | async-start | bytes 7077888 | tf_op jit(solution)/shard_map/all_gather | solution.py:21
  9.4 506.6 %reduce-scatter.2.cloned.1.call-start = ((), (), s32[]{:S(2)}) async-start(), calls=%async_computation.5 | async-start | bytes 13369344 | tf_op jit(solution)/shard_map/reduce_scatter | solution.py:54
  12.0 3.3 copy-start
  12.0 99.7 %copy-start.3 = (f32[2048]{0:T(1024)S(1)}, f32[2048]{0:T(1024)}, u32[]{:S(2)}) copy-start(f32[2048]{0:T(1024)} %param.7) | copy-start | bytes 24580
  210.7 7.5 %copy-start.2 = (bf16[512,2,8,128]{0,3,2,1:T(8,128)(2,1)S(1)}, bf16[512,2,8,128]{0,3,2,1:T(8,128)(2,1)}, u32[]{:S(2)}) copy-start(bf16[512,2,8,128]{0,3,2,1:T(8,128)(2,1)} %copy.12) | copy-start | bytes 6291460
  210.7 7.5 %copy-start.4 = (f32[512,1536]{1,0:T(8,128)S(1)}, f32[512,1536]{1,0:T(8,128)}, u32[]{:S(2)}) copy-start(f32[512,1536]{1,0:T(8,128)} %fusion.14) | copy-start | bytes 9437188
  216.5 1.8 copy-start.6
  225.1 314.5 %all-reduce.2.cloned.1.call-start = ((), (), s32[]{:S(2)}) async-start(), calls=%async_computation.4 | async-start | bytes 4194304 | tf_op jit(solution)/shard_map/psum | solution.py:35
  309.8 8.6 %copy-start.5 = (f32[512,1536]{1,0:T(8,128)S(1)}, f32[512,1536]{1,0:T(8,128)}, u32[]{:S(2)}) copy-start(f32[512,1536]{1,0:T(8,128)} %fusion.14) | copy-start | bytes 9437188
  309.8 8.6 %copy-start.7 = (f32[512,1536]{1,0:T(8,128)S(1)}, f32[512,1536]{1,0:T(8,128)}, u32[]{:S(2)}) copy-start(f32[512,1536]{1,0:T(8,128)} %copy-done.6) | copy-start | bytes 9437188
  309.8 17.2 %slice-start = ((s8[6291456]{0:T(1024)(128)(4,1)}), s8[4194304]{0:T(1024)(128)(4,1)S(1)}, s32[]{:S(2)}) async-start(s8[6291456]{0:T(1024)(128)(4,1)} %bitcast.15), calls=%async_computation.7 | async-start | bytes 8388608
  318.4 8.6 %slice-start.1 = ((s8[6291456]{0:T(1024)(128)(4,1)}), s8[2097152]{0:T(1024)(128)(4,1)S(1)}, s32[]{:S(2)}) async-start(s8[6291456]{0:T(1024)(128)(4,1)} %bitcast.15), calls=%async_computation.8 | async-start | bytes 4194304
  333.7 257.1 %all-gather.11.cloned.1.call-start = ((), (), s32[]{:S(2)}) async-start(), calls=%async_computation.6 | async-start | bytes 2359296 | tf_op jit(solution)/shard_map/all_gather | solution.py:60
Sparse Core Ops, SparseCore 0:
  10.2 101.4 all-gather.8
  113.8 96.8 all-gather.6
  212.9 96.8 all-gather.4
  315.3 200.6 reduce-scatter.1
  518.8 20.7 all-reduce.1
  541.0 28.3 all-gather.10
where the time goes:
time: 601 us
  waiting for transfers between devices  480 us (80%)
  matrix products  44.2 us (7%)
  blocking collectives  43.3 us (7%)
  between operations  14.2 us (2%)
  local copies, waits for them, and re-layouts  10.6 us (2%)
  other arithmetic  8.39 us (1%)
    reduce_scatter x1, waiting for transfers between devices, local(): lax.psum_scatter(0.5 * lax.dot_general(reordered, hidden, contract_rows,...  182 us
    all_gather x1, waiting for transfers between devices, local(): lax.all_gather(gate_weight, 'fs', axis=0, tiled=True)  95.9 us
    all_gather x1, waiting for transfers between devices, local(): lax.all_gather(up_weight, 'fs', axis=0, tiled=True)  91.2 us
    all_gather x1, waiting for transfers between devices, local(): lax.all_gather(down_weight, 'fs', axis=0, tiled=True)  84.5 us
    psum x1, blocking collectives, local(): lax.psum(jnp.sum(normalized_gradient * unit_input, axis=0), ('rep', 'fs'))  43.3 us
    psum x1, waiting for transfers between devices, local(): summed_units = lax.psum(partial_value.astype(jnp.bfloat16), 'tp')  23.6 us
  transfers between devices with their start and end apart: 6, of which 5 were waited for; matrix products, arithmetic and copies ran while one was open for 10% of the time, Pallas kernels for 0%

commit v1 on v0

v1 whole, which is shorter than its diff:
```python
import jax
import jax.numpy as jnp
from jax import lax
from jax.sharding import PartitionSpec as P

EPS = 1e-06


def shift(value, axis, step):
    size = lax.axis_size(axis)
    return lax.ppermute(value, axis, [(i, (i + step) % size) for i in range(size)])


def local(inputs, gain, gate_weight, up_weight, down_weight, cotangent):
    n_rep, n_tp = lax.axis_size("rep"), lax.axis_size("tp")
    rep, tp = lax.axis_index("rep"), lax.axis_index("tp")
    rows, width = inputs.shape
    block = rows // n_tp
    units = gate_weight.shape[1] // n_rep

    def own_units(weight):
        return lax.dynamic_slice_in_dim(weight, rep * units, units, axis=1)

    def own_block(value, step):
        return lax.dynamic_slice_in_dim(value, (tp + step) % n_tp * block, block, axis=0)

    def gathered_tokens(value):
        parts = [own_block(value, s) for s in range(n_tp)]
        for j in range(1, n_rep):
            first = shift(own_block(value, 0), "rep", -j)
            parts += [first] + [shift(first, "tp", -s) for s in range(1, n_tp)]
        return jnp.concatenate(parts, axis=0)

    gate_full = lax.all_gather(own_units(gate_weight), "fs", axis=0, tiled=True)
    up_full = lax.all_gather(own_units(up_weight), "fs", axis=0, tiled=True)
    down_full = lax.all_gather(own_units(down_weight), "fs", axis=0, tiled=True)

    tokens = gathered_tokens(inputs)
    cots = gathered_tokens(cotangent)

    def normed(value):
        single = value.astype(jnp.float32)
        inv = lax.rsqrt(jnp.mean(single * single, axis=-1, keepdims=True) + EPS)
        return single * inv, inv

    normalized_input = (normed(tokens)[0] * gain).astype(jnp.bfloat16)
    contract_cols = (((1,), (1,)), ((), ()))
    contract_rows = (((0,), (0,)), ((), ()))
    gate = jnp.dot(normalized_input, gate_full, preferred_element_type=jnp.float32)
    up_proj = jnp.dot(normalized_input, up_full, preferred_element_type=jnp.float32)
    gate_sig = jax.nn.sigmoid(gate)
    active = gate * gate_sig
    hidden = (active * up_proj).astype(jnp.bfloat16)
    summed = lax.psum_scatter(
        (0.5 * lax.dot_general(cots, hidden, contract_rows, preferred_element_type=jnp.float32)).astype(jnp.bfloat16),
        "fs",
        scatter_dimension=0,
        tiled=True,
    )
    d_hidden = 0.5 * jnp.dot(cots, down_full, preferred_element_type=jnp.float32)
    d_gate = (d_hidden * up_proj * gate_sig * (1.0 + gate * (1.0 - gate_sig))).astype(jnp.bfloat16)
    d_up = (d_hidden * active).astype(jnp.bfloat16)
    partial_value = (
        lax.dot_general(d_gate, gate_full, contract_cols, preferred_element_type=jnp.float32)
        + lax.dot_general(d_up, up_full, contract_cols, preferred_element_type=jnp.float32)
    ).astype(jnp.bfloat16).reshape(n_rep, n_tp, block, width)
    over_tp = partial_value[:, 0].astype(jnp.float32)
    for s in range(1, n_tp):
        over_tp = over_tp + shift(partial_value[:, s], "tp", s).astype(jnp.float32)
    over_tp = over_tp.astype(jnp.bfloat16)
    total = over_tp[0].astype(jnp.float32)
    for j in range(1, n_rep):
        total = total + shift(over_tp[j], "rep", j).astype(jnp.float32)
    normalized_gradient = total.astype(jnp.bfloat16).astype(jnp.float32)
    unit_input, inv = normed(own_block(inputs, 0))
    gain_gradient = lax.psum(
        jnp.sum(normalized_gradient * unit_input, axis=0), ("rep", "fs", "tp")
    )
    gain_scaled = gain * normalized_gradient
    mean_correction = jnp.mean(gain_scaled * unit_input, axis=-1, keepdims=True)
    block_gradient = (
        own_block(cotangent, 0).astype(jnp.float32)
        + inv * (gain_scaled - unit_input * mean_correction)
    ).astype(jnp.bfloat16)
    input_gradient = jnp.zeros((rows, width), jnp.bfloat16)
    for s in range(n_tp):
        piece = block_gradient if s == 0 else shift(block_gradient, "tp", -s)
        input_gradient = lax.dynamic_update_slice_in_dim(
            input_gradient, piece, (tp + s) % n_tp * block, axis=0
        )
    d_down = jnp.zeros((summed.shape[0], units * n_rep), jnp.float32)
    for j in range(n_rep):
        piece = summed if j == 0 else shift(summed, "rep", -j)
        d_down = lax.dynamic_update_slice_in_dim(
            d_down, piece.astype(jnp.float32), (rep + j) % n_rep * units, axis=1
        )
    return (input_gradient, gain_gradient, d_down)


def solution(mesh):
    placed = (
        P(("rep", "fs"), None),
        P(),
        P("fs", "tp"),
        P("fs", "tp"),
        P("fs", "tp"),
        P(("rep", "fs"), None),
    )
    return jax.shard_map(
        local,
        mesh=mesh,
        in_specs=placed,
        out_specs=(P(("rep", "fs"), None), P(), P("fs", "tp")),
        check_vma=False,
    )
```

time: 601 us -> 323 us (0.54)
  waiting for transfers between devices: 480 us -> 185 us
  local copies, waits for them, and re-layouts: 10.6 us -> 18.6 us
    reduce_scatter x1, waiting for transfers between devices: 182 us -> 0.72 us  [local(): lax.psum_scatter((0.5 * lax.dot_general(cots, hidden, contract_rows, pref...]
    all_gather x4 -> x3, waiting for transfers between devices: 272 us -> 110 us  [the longest x1 52.3 us: local(): gate_full = lax.all_gather(own_units(gate_weight), 'fs', axis=0, tiled=True)]
    ppermute x0 -> x8, waiting for transfers between devices: none -> 74.6 us  [shift(): lax.ppermute(value, axis, [(i, (i + step) % size) for i in range(size)])]
    psum x1 -> x0, waiting for transfers between devices: 23.6 us -> none  [local(): summed_units = lax.psum(partial_value.astype(jnp.bfloat16), 'tp')]
    dynamic_slice x0 -> x5, local copies, waits for them, and re-layouts: none -> 7.3 us  [the longest x3 4.36 us: own_units(): return lax.dynamic_slice_in_dim(weight, rep * units, units, axis=1)]
    ppermute x0 -> x8, starting transfers between devices: none -> 6.14 us  [shift(): lax.ppermute(value, axis, [(i, (i + step) % size) for i in range(size)])]
  transfers between devices with their start and end apart: 6 -> 12, of which waited for: 5 -> 8; matrix products, arithmetic and copies ran while one was open for 10% -> 14% of each run, Pallas kernels for 0% -> 0%
where the time goes in v1:
time: 323 us
  waiting for transfers between devices  185 us (57%)
  matrix products  48.5 us (15%)
  blocking collectives  39.6 us (12%)
  local copies, waits for them, and re-layouts  18.6 us (6%)
  between operations  14 us (4%)
  other arithmetic  10.6 us (3%)
  starting transfers between devices  6.31 us (2%)
    ppermute x8, waiting for transfers between devices, shift(): lax.ppermute(value, axis, [(i, (i + step) % size) for i in range(size)])  74.6 us
    all_gather x1, waiting for transfers between devices, local(): gate_full = lax.all_gather(own_units(gate_weight), 'fs', axis=0, tiled=True)  52.3 us
    all_gather x1, waiting for transfers between devices, local(): down_full = lax.all_gather(own_units(down_weight), 'fs', axis=0, tiled=True)  51.7 us
    psum x1, blocking collectives, local(): lax.psum(jnp.sum(normalized_gradient * unit_input, axis=0), ('rep', 'fs',...  39.6 us
    dot_general x1, matrix products, local(): jnp.dot(normalized_input, gate_full, preferred_element_type=jnp.float32)  9.21 us
    dot_general x1, matrix products, local(): jnp.dot(normalized_input, up_full, preferred_element_type=jnp.float32)  9.2 us
    unnamed x34, local copies, waits for them, and re-layouts  8.26 us
    dot_general x1, matrix products, local(): jnp.dot(cots, down_full, preferred_element_type=jnp.float32)  7.95 us
  transfers between devices with their start and end apart: 12, of which 8 were waited for; matrix products, arithmetic and copies ran while one was open for 14% of the time, Pallas kernels for 0%

profile of v1, /device:TPU:0, one launch (start us, length us, event | category | flops | bytes accessed | tf_op | source)
XLA Modules:
  0.0 322.7 jit_solution(815595748721694349)
XLA Ops:
  7.2 1.1 copy-done
  9.2 1.8 constant_dynamic-slice_fusion
  11.0 1.8 constant_dynamic-slice_fusion.3
  12.9 1.5 fusion.12
  14.4 3.0 collective-permute-start.2
  17.4 2.9 constant_dynamic-slice_fusion.4
  20.4 21.2 %collective-permute-done.2 = bf16[256,2048]{1,0:T(8,128)(2,1)} collective-permute-done((bf16[256,2048]{1,0:T(8,128)(2,1)S(1)}, bf16[256,2048]{1,0:T(8,128)(2,1)}, u32[]{:S(2)}, u32[]{:S(2)}) %collective-permute-start.2) | collective-permute-done | bytes 1048608 | tf_op jit(solution)/shard_map/ppermute | solution.py:11
  41.7 21.5 %collective-permute-done = bf16[256,2048]{1,0:T(8,128)(2,1)} collective-permute-done((bf16[256,2048]{1,0:T(8,128)(2,1)S(1)}, bf16[256,2048]{1,0:T(8,128)(2,1)}, u32[]{:S(2)}, u32[]{:S(2)}) %collective-permute-start) | collective-permute-done | bytes 1048608 | tf_op jit(solution)/shard_map/ppermute | solution.py:11
  63.2 1.0 copy-done.8
  64.2 3.0 fusion
  67.1 5.8 %all-gather.6.cloned.1.call-done = bf16[2048,768]{1,0:T(8,128)(2,1)} async-done(((bf16[256,768]{1,0:T(8,128)(2,1)}), bf16[2048,768]{1,0:T(8,128)(2,1)}) %all-gather.6.cloned.1.call-update) | async-done | bytes 3145744 | tf_op jit(solution)/shard_map/all_gather | solution.py:35
  72.9 9.2 %fusion.21 = f32[1024,768]{1,0:T(8,128)} fusion(bf16[2048,768]{1,0:T(8,128)(2,1)} %all-gather.6.cloned.1.call-done, f32[2048]{0:T(1024)S(1)} %copy-done.10, f32[1024]{0:T(1024)S(1)} %add_rsqrt_fusion, bf16[256,2048]{1,0:T(8,128)(2,1)} %copy-done.8, bf16[256,2048]{1,0:T(8,128)(2,1)} %collective-permute-done.2, ...), kind=kOutput, calls=%fused_computation.38 | convolution fusion | flops 3244294144 | bytes 10498048 | tf_op jit(solution)/shard_map/dot_general | solution.py:50
  82.2 52.3 %all-gather.8.cloned.1.call-done = bf16[2048,768]{1,0:T(8,128)(2,1)} async-done(((bf16[256,768]{1,0:T(8,128)(2,1)}), bf16[2048,768]{1,0:T(8,128)(2,1)}) %all-gather.8.cloned.1.call-update) | async-done | bytes 3145744 | tf_op jit(solution)/shard_map/all_gather | solution.py:34
  134.4 9.2 %fusion.19 = f32[1024,768]{1,0:T(8,128)} fusion(bf16[2048,768]{1,0:T(8,128)(2,1)} %all-gather.8.cloned.1.call-done, f32[2048]{0:T(1024)S(1)} %copy-done.10, f32[1024]{0:T(1024)S(1)} %add_rsqrt_fusion, bf16[256,2048]{1,0:T(8,128)(2,1)} %copy-done.8, bf16[256,2048]{1,0:T(8,128)(2,1)} %collective-permute-done.2, ...), kind=kOutput, calls=%fused_computation.37 | convolution fusion | flops 3244294144 | bytes 10498048 | tf_op jit(solution)/shard_map/dot_general | solution.py:49
  143.6 51.7 %all-gather.4.cloned.1.call-done = bf16[2048,768]{1,0:T(8,128)(2,1)} async-done(((bf16[256,768]{1,0:T(8,128)(2,1)}), bf16[2048,768]{1,0:T(8,128)(2,1)}) %all-gather.4.cloned.1.call-update) | async-done | bytes 3145744 | tf_op jit(solution)/shard_map/all_gather | solution.py:36
  195.3 7.9 %fusion.23 = f32[1024,768]{1,0:T(8,128)S(1)} fusion(bf16[2048,768]{1,0:T(8,128)(2,1)} %all-gather.4.cloned.1.call-done, bf16[256,2048]{1,0:T(8,128)(2,1)} %collective-permute-done.1, bf16[256,2048]{1,0:T(8,128)(2,1)} %collective-permute-done, bf16[256,2048]{1,0:T(8,128)(2,1)} %get-tuple-element.9, bf16[256,2048]{1,0:T(8,128)(2,1)} %copy-done.2), kind=kOutput, calls=%fused_computation.43 | convolution fusion | flops 3238002688 | bytes 10485760 | tf_op jit(solution)/shard_map/dot_general | solution.py:60
  203.3 1.6 copy-done.14
  204.9 7.4 %fusion.15 = f32[1024,2048]{1,0:T(8,128)} fusion(bf16[2048,768]{1,0:T(8,128)(2,1)S(1)} %copy-done.12, f32[1024,768]{1,0:T(8,128)S(1)} %copy-done.13, f32[1024,768]{1,0:T(8,128)S(1)} %copy-done.15, f32[1024,768]{1,0:T(8,128)S(1)} %fusion.23), kind=kOutput, calls=%fused_computation.33 | convolution fusion | flops 3229876224 | bytes 20971520 | tf_op jit(solution)/shard_map/dot_general | solution.py:64
  212.3 7.6 %add_convert_fusion = bf16[1024,2048]{1,0:T(8,128)(2,1)S(1)} fusion(f32[1024,2048]{1,0:T(8,128)} %fusion.15, bf16[2048,768]{1,0:T(8,128)(2,1)S(1)} %copy-done.11, f32[1024,768]{1,0:T(8,128)} %copy-done.14, f32[1024,768]{1,0:T(8,128)S(1)} %copy-done.13), kind=kOutput, calls=%fused_computation.5 | convolution fusion | flops 3230924800 | bytes 22020096 | tf_op jit(solution)/shard_map/dot_general | solution.py:65
  220.0 2.1 copy-done.1
  222.1 1.5 slice_bitcast_fusion
  223.6 7.0 %multiply_convert_fusion = bf16[2048,768]{1,0:T(8,128)(2,1)} fusion(f32[1024,768]{1,0:T(8,128)S(1)} %copy-done.16, bf16[256,2048]{1,0:T(8,128)(2,1)} %collective-permute-done.1, bf16[256,2048]{1,0:T(8,128)(2,1)} %collective-permute-done, bf16[256,2048]{1,0:T(8,128)(2,1)S(1)} %copy-done.7, bf16[256,2048]{1,0:T(8,128)(2,1)S(1)} %copy-done.3, ...), kind=kOutput, calls=%fused_computation.6 | convolution fusion | flops 3245867008 | bytes 13631488 | tf_op jit(solution)/shard_map/dot_general | solution.py:55
  230.7 3.0 fusion.3
  233.8 1.5 collective-permute-start.5
  235.3 24.1 %collective-permute-done.5 = bf16[256,2048]{1,0:T(8,128)(2,1)S(1)} collective-permute-done((bf16[256,2048]{1,0:T(8,128)(2,1)S(1)}, bf16[256,2048]{1,0:T(8,128)(2,1)S(1)}, u32[]{:S(2)}, u32[]{:S(2)}) %collective-permute-start.5) | collective-permute-done | bytes 1048608 | tf_op jit(solution)/shard_map/ppermute | solution.py:11
  260.5 2.1 constant_dynamic-update-slice_fusion.1
  262.6 1.3 copy-done.5
  263.9 39.6 %psum.7 = f32[2048]{0:T(1024)} all-reduce(f32[2048]{0:T(1024)S(1)} %get-tuple-element.3), channel_id=1, replica_groups=mesh['rep'=2,'fs'=8,'tp'=2] {'rep','fs','tp'}, use_global_device_ids=true, to_apply=%region_4.5 | all-reduce | flops 2048 | bytes 16384 | tf_op jit(solution)/shard_map/psum | solution.py:76
  304.2 1.6 collective-permute-start.7
  305.8 1.0 constant_dynamic-update-slice_fusion
  307.1 7.8 %collective-permute-done.7 = bf16[256,768]{1,0:T(8,128)(2,1)S(1)} collective-permute-done((bf16[256,768]{1,0:T(8,128)(2,1)}, bf16[256,768]{1,0:T(8,128)(2,1)S(1)}, u32[]{:S(2)}, u32[]{:S(2)}) %collective-permute-start.7) | collective-permute-done | bytes 393248 | tf_op jit(solution)/shard_map/ppermute | solution.py:11
  315.0 1.1 copy-done.6
  (57 shorter events, 3.5 us)
Async XLA Ops:
  7.2 1.1 copy-start
  7.2 65.8 %all-gather.6.cloned.1.call-start = ((), (), s32[]{:S(2)}) async-start(), calls=%async_computation.2 | async-start | bytes 3538944 | tf_op jit(solution)/shard_map/all_gather | solution.py:35
  9.1 125.3 %all-gather.8.cloned.1.call-start = ((), (), s32[]{:S(2)}) async-start(), calls=%async_computation.3 | async-start | bytes 3538944 | tf_op jit(solution)/shard_map/all_gather | solution.py:34
  11.0 184.3 %all-gather.4.cloned.1.call-start = ((), (), s32[]{:S(2)}) async-start(), calls=%async_computation.1 | async-start | bytes 3538944 | tf_op jit(solution)/shard_map/all_gather | solution.py:36
  12.8 291.4 %reduce-scatter.2.cloned.1.call-start = ((), (), s32[]{:S(2)}) async-start(), calls=%async_computation.4 | async-start | bytes 3538944 | tf_op jit(solution)/shard_map/reduce_scatter | solution.py:54
  14.4 27.1 %collective-permute-start.2 = (bf16[256,2048]{1,0:T(8,128)(2,1)S(1)}, bf16[256,2048]{1,0:T(8,128)(2,1)}, u32[]{:S(2)}, u32[]{:S(2)}) collective-permute-start(bf16[256,2048]{1,0:T(8,128)(2,1)S(1)} %get-tuple-element.8), channel_id=1, source_target_pairs={{0,16},{16,0},{1,17},{17,1},{2,18},{18,2},{3,19},{19,3},{4,20},{20... | collective-permute-start | bytes 3145736 | tf_op jit(solution)/shard_map/ppermute | solution.py:11
  17.4 24.1 %copy-start.4 = (bf16[512,2048]{1,0:T(8,128)(2,1)S(1)}, bf16[512,2048]{1,0:T(8,128)(2,1)}, u32[]{:S(2)}) copy-start(bf16[512,2048]{1,0:T(8,128)(2,1)} %param.6) | copy-start | bytes 6291460
  20.3 21.3 %copy-start.2 = (bf16[256,2048]{1,0:T(8,128)(2,1)}, bf16[256,2048]{1,0:T(8,128)(2,1)S(1)}, u32[]{:S(2)}) copy-start(bf16[256,2048]{1,0:T(8,128)(2,1)S(1)} %get-tuple-element.10) | copy-start | bytes 3145732
  20.3 52.6 %copy-start.10 = (f32[2048]{0:T(1024)S(1)}, f32[2048]{0:T(1024)}, u32[]{:S(2)}) copy-start(f32[2048]{0:T(1024)} %param.7) | copy-start | bytes 24580
  20.3 42.9 %collective-permute-start = (bf16[256,2048]{1,0:T(8,128)(2,1)S(1)}, bf16[256,2048]{1,0:T(8,128)(2,1)}, u32[]{:S(2)}, u32[]{:S(2)}) collective-permute-start(bf16[256,2048]{1,0:T(8,128)(2,1)S(1)} %get-tuple-element.10), channel_id=1, source_target_pairs={{0,16},{16,0},{1,17},{17,1},{2,18},{18,2},{3,19},{19,3},{4,20},{20... | collective-permute-start | bytes 3145736 | tf_op jit(solution)/shard_map/ppermute | solution.py:11
  41.6 21.6 %collective-permute-start.3 = (bf16[256,2048]{1,0:T(8,128)(2,1)}, bf16[256,2048]{1,0:T(8,128)(2,1)S(1)}, u32[]{:S(2)}, u32[]{:S(2)}) collective-permute-start(bf16[256,2048]{1,0:T(8,128)(2,1)} %collective-permute-done.2), channel_id=1, source_target_pairs={{0,1},{1,0},{2,3},{3,2},{4,5},{5,4},{6,7},{7,6},{8,9},{9,8},{10,11... | collective-permute-start | bytes 3145736 | tf_op jit(solution)/shard_map/ppermute | solution.py:11
  63.2 80.4 %collective-permute-start.1 = (bf16[256,2048]{1,0:T(8,128)(2,1)}, bf16[256,2048]{1,0:T(8,128)(2,1)}, u32[]{:S(2)}, u32[]{:S(2)}) collective-permute-start(bf16[256,2048]{1,0:T(8,128)(2,1)} %collective-permute-done), channel_id=1, source_target_pairs={{0,1},{1,0},{2,3},{3,2},{4,5},{5,4},{6,7},{7,6},{8,9},{9,8},{10,11... | collective-permute-start | bytes 3145736 | tf_op jit(solution)/shard_map/ppermute | solution.py:11
  63.2 1.0 copy-start.8
  195.3 9.6 %copy-start.12 = (bf16[2048,768]{1,0:T(8,128)(2,1)S(1)}, bf16[2048,768]{1,0:T(8,128)(2,1)}, u32[]{:S(2)}) copy-start(bf16[2048,768]{1,0:T(8,128)(2,1)} %all-gather.8.cloned.1.call-done) | copy-start | bytes 9437188
  195.3 9.6 %copy-start.13 = (f32[1024,768]{1,0:T(8,128)S(1)}, f32[1024,768]{1,0:T(8,128)}, u32[]{:S(2)}) copy-start(f32[1024,768]{1,0:T(8,128)} %fusion.19) | copy-start | bytes 9437188
  195.3 9.6 %copy-start.15 = (f32[1024,768]{1,0:T(8,128)S(1)}, f32[1024,768]{1,0:T(8,128)}, u32[]{:S(2)}) copy-start(f32[1024,768]{1,0:T(8,128)} %fusion.21) | copy-start | bytes 9437188
  203.3 1.6 copy-start.14
  204.9 7.4 %copy-start.11 = (bf16[2048,768]{1,0:T(8,128)(2,1)S(1)}, bf16[2048,768]{1,0:T(8,128)(2,1)}, u32[]{:S(2)}) copy-start(bf16[2048,768]{1,0:T(8,128)(2,1)} %all-gather.6.cloned.1.call-done) | copy-start | bytes 9437188
  212.3 11.3 %copy-start.16 = (f32[1024,768]{1,0:T(8,128)S(1)}, f32[1024,768]{1,0:T(8,128)}, u32[]{:S(2)}) copy-start(f32[1024,768]{1,0:T(8,128)} %fusion.21) | copy-start | bytes 9437188
  220.0 2.1 copy-start.1
  220.0 3.6 %copy-start.3 = (bf16[256,2048]{1,0:T(8,128)(2,1)S(1)}, bf16[256,2048]{1,0:T(8,128)(2,1)}, u32[]{:S(2)}) copy-start(bf16[256,2048]{1,0:T(8,128)(2,1)} %copy-done.2) | copy-start | bytes 3145732
  220.0 3.6 %copy-start.7 = (bf16[256,2048]{1,0:T(8,128)(2,1)S(1)}, bf16[256,2048]{1,0:T(8,128)(2,1)}, u32[]{:S(2)}) copy-start(bf16[256,2048]{1,0:T(8,128)(2,1)} %get-tuple-element.9) | copy-start | bytes 3145732
  223.6 7.1 %collective-permute-start.4 = (bf16[2,256,2048]{2,1,0:T(8,128)(2,1)}, bf16[2,256,2048]{2,1,0:T(8,128)(2,1)}, u32[]{:S(2)}, u32[]{:S(2)}) collective-permute-start(bf16[2,256,2048]{2,1,0:T(8,128)(2,1)} %slice_bitcast_fusion), channel_id=1, source_target_pairs={{0,1},{1,0},{2,3},{3,2},{4,5},{5,4},{6,7},{7,6},{8,9},{9,8},{10,11... | collective-permute-start | bytes 6291464 | tf_op jit(solution)/shard_map/ppermute | solution.py:11
  233.8 25.6 %collective-permute-start.5 = (bf16[256,2048]{1,0:T(8,128)(2,1)S(1)}, bf16[256,2048]{1,0:T(8,128)(2,1)S(1)}, u32[]{:S(2)}, u32[]{:S(2)}) collective-permute-start(bf16[256,2048]{1,0:T(8,128)(2,1)S(1)} %slice_bitcast_fusion.2), channel_id=1, source_target_pairs={{0,16},{16,0},{1,17},{17,1},{2,18},{18,2},{3,19},{19,3},{4,20},{20... | collective-permute-start | bytes 3145736 | tf_op jit(solution)/shard_map/ppermute | solution.py:11
  262.6 1.3 copy-start.5
  263.9 41.9 %collective-permute-start.6 = (bf16[256,2048]{1,0:T(8,128)(2,1)}, bf16[256,2048]{1,0:T(8,128)(2,1)S(1)}, u32[]{:S(2)}, u32[]{:S(2)}) collective-permute-start(bf16[256,2048]{1,0:T(8,128)(2,1)} %get-tuple-element.6), channel_id=1, source_target_pairs={{0,1},{1,0},{2,3},{3,2},{4,5},{5,4},{6,7},{7,6},{8,9},{9,8},{10,11... | collective-permute-start | bytes 3145736 | tf_op jit(solution)/shard_map/ppermute | solution.py:11
  304.2 2.8 copy-start.9
  304.2 10.6 %collective-permute-start.7 = (bf16[256,768]{1,0:T(8,128)(2,1)}, bf16[256,768]{1,0:T(8,128)(2,1)S(1)}, u32[]{:S(2)}, u32[]{:S(2)}) collective-permute-start(bf16[256,768]{1,0:T(8,128)(2,1)} %reduce-scatter.2.cloned.1.call-done), channel_id=1, source_target_pairs={{0,16},{16,0},{1,17},{17,1},{2,18},{18,2},{3,19},{19,3},{4,20},{20... | collective-permute-start | bytes 1179656 | tf_op jit(solution)/shard_map/ppermute | solution.py:11
  315.0 1.1 copy-start.6
Sparse Core Ops, SparseCore 0:
  10.2 62.7 all-gather.5
  75.7 58.6 all-gather.7
  136.6 58.6 all-gather.3
  230.8 73.4 reduce-scatter.1
